TPU v7x, 32 devices: a whole 2x2x4 slice. The times are simulated.
32 devices in a mesh: gr: 2 (over y), sp: 4 (over z), tp: 4 (over x, core).
Axes of the slice: x: 2, y: 2, z: 4, core: 2. Of those that a mesh axis runs over, the one named last changes fastest.
Arguments:
- layer_input: bfloat16 [2, 3072, 2048], P('gr', ('sp', 'tp')), may hold values from -6 to 6
- key_weight: bfloat16 [2048, 2048], P(None, 'tp'), may hold values from -0.125 to 0.125
- value_weight: bfloat16 [2048, 2048], P(None, 'tp'), may hold values from -0.125 to 0.125
- new_queries: bfloat16 [2, 2048], P('gr', 'tp'), may hold values from -280 to 280
- lambdas: float32 [16], P('tp'), may hold values from 0.3 to 0.8
- head_gain: float32 [128], replicated, may hold values from 0.1 to 1.9
- out_weight: bfloat16 [2048, 2048], P('tp'), may hold values from -0.125 to 0.125
Outputs:
- key_cache: bfloat16 [2, 3072, 2048], P('gr', 'sp', 'tp')
- value_cache: bfloat16 [2, 3072, 2048], P('gr', 'sp', 'tp')
- mixed: bfloat16 [2, 2048], P('gr', 'tp')
All inputs are finite; a program needn't handle non-finite values.
Results may differ from a plain program's by a relative error of at most 0.03.
Values may be sent and summed in bfloat16 or wider, within the bound.
A program may use at most 64 MiB of HBM per device.

v0:
```python
import jax
import jax.numpy as jnp
from jax import lax
from jax.sharding import PartitionSpec as P


def rotate(raw_keys, positions, head_dim):
    inverse = 1.0 / 10000.0 ** (jnp.arange(0, head_dim, 2, dtype=jnp.float32) / head_dim)
    angles = positions.astype(jnp.float32)[:, None] * inverse[None, :]
    angles = jnp.concatenate([angles, angles], axis=-1)
    cosine = jnp.cos(angles)[:, None, :]
    sine = jnp.sin(angles)[:, None, :]
    first_half, second_half = jnp.split(raw_keys, 2, axis=-1)
    turned = jnp.concatenate([-second_half, first_half], axis=-1)
    return raw_keys * cosine + turned * sine


def partial_read(queries, key_rows, value_rows, heads_here, head_dim):
    seq_count = queries.shape[0]
    queries_wide = queries.reshape(seq_count, heads_here, 2, head_dim)
    keys_wide = key_rows.reshape(seq_count, -1, heads_here, 2, head_dim)
    scores = jnp.einsum(
        "shmd,slhmd->shml", queries_wide, keys_wide, preferred_element_type=jnp.float32
    )
    scores = scores * head_dim ** (-0.5)
    highest = jnp.max(scores, axis=-1)
    weights = jnp.exp(scores - highest[..., None])
    totals = jnp.sum(weights, axis=-1)
    values_wide = value_rows.reshape(seq_count, -1, heads_here, 2 * head_dim).astype(jnp.float32)
    weighted = jnp.einsum("shml,slhe->shme", weights, values_wide)
    return (highest, totals, weighted)


def finish(totals, weighted, lambdas, head_gain):
    reads = weighted / totals[..., None]
    diff = reads[:, :, 0] - lambdas[None, :, None] * reads[:, :, 1]
    normed = diff * lax.rsqrt(jnp.mean(diff * diff, axis=-1, keepdims=True) + 1e-06) * head_gain
    return normed.reshape(normed.shape[0], -1).astype(jnp.bfloat16)


def on_device(layer_input, key_weight, value_weight, new_queries, lambdas, head_gain, out_weight):
    heads_here = lambdas.shape[0]
    column_count = key_weight.shape[1]
    head_dim = column_count // (2 * heads_here)
    rows_here = layer_input.shape[1]
    first_position = lax.axis_index("sp") * (rows_here * lax.axis_size("tp"))
    piece = lax.all_gather(layer_input, "tp", axis=1, tiled=True)
    seq_count = piece.shape[0]
    count = piece.shape[1]
    flattened = piece.reshape(seq_count * count, piece.shape[2])
    raw_keys = jnp.dot(flattened, key_weight, preferred_element_type=jnp.float32)
    raw_values = jnp.dot(flattened, value_weight, preferred_element_type=jnp.float32)
    positions = first_position + jnp.arange(count, dtype=jnp.int32)
    turned_keys = rotate(
        raw_keys.reshape(seq_count, count, 2 * heads_here, head_dim), positions, head_dim
    )
    key_part = turned_keys.reshape(seq_count, count, column_count).astype(jnp.bfloat16)
    value_part = raw_values.reshape(seq_count, count, column_count).astype(jnp.bfloat16)
    both = jnp.concatenate([key_part, value_part], axis=2)
    key_rows = both[:, :, :column_count]
    value_rows = both[:, :, column_count:]
    highest, totals, weighted = partial_read(
        new_queries, key_rows, value_rows, heads_here, head_dim
    )
    overall = lax.pmax(highest, "sp")
    factor = jnp.exp(highest - overall)
    totals, weighted = lax.psum((totals * factor, weighted * factor[..., None]), "sp")
    headed = finish(totals, weighted, lambdas, head_gain)
    partials = jnp.dot(headed, out_weight, preferred_element_type=jnp.float32)
    partials = partials.astype(jnp.bfloat16).astype(jnp.float32)
    mixed = lax.psum_scatter(partials.astype(jnp.bfloat16), "tp", scatter_dimension=1, tiled=True)
    return (key_rows, value_rows, mixed)


def solution(mesh):
    in_specs = (
        P("gr", ("sp", "tp"), None),
        P(None, "tp"),
        P(None, "tp"),
        P("gr", "tp"),
        P("tp"),
        P(),
        P("tp", None),
    )
    out_specs = (P("gr", "sp", "tp"), P("gr", "sp", "tp"), P("gr", "tp"))
    return jax.shard_map(
        on_device, mesh=mesh, in_specs=in_specs, out_specs=out_specs, check_vma=False
    )
```

profile of v0, /device:TPU:0, one launch (start us, length us, event | category | flops | bytes accessed | tf_op | source)
XLA Modules:
  0.0 104.3 jit_solution(5263572090222593058)
XLA Ops:
  7.2 0.0 copy-start
  7.2 0.0 all-gather.2.cloned.1.call-start
  7.2 0.7 all-gather.2.cloned.1.call-update
  7.9 0.0 reduce-scatter.4.cloned.1.call-start
  8.0 0.7 reduce.5
  8.7 0.1 reshape.247
  8.8 0.1 broadcast_multiply_fusion
  8.8 0.4 fusion.11
  9.2 31.6 %all-gather.2.cloned.1.call-done = bf16[1,768,2048]{2,1,0:T(8,128)(2,1)} async-done(((bf16[1,192,2048]{2,1,0:T(8,128)(2,1)}), bf16[1,768,2048]{2,1,0:T(8,128)(2,1)}) %all-gather.2.cloned.1.call-update) | async-done | bytes 3145744 | tf_op jit(solution)/shard_map/all_gather | solution.py:47
  40.8 0.0 copy-done
  40.8 3.7 %fusion.2 = f32[768,512]{0,1:T(8,128)S(1)} fusion(bf16[2048,512]{1,0:T(8,128)(2,1)S(1)} %copy-done, bf16[1,768,2048]{2,1,0:T(8,128)(2,1)} %all-gather.2.cloned.1.call-done), kind=kOutput, calls=%fused_computation.2 | convolution fusion | flops 1610612736 | bytes 6815744 | tf_op jit(solution)/shard_map/dot_general | solution.py:51
  44.5 0.1 slice_negate_fusion
  44.7 0.1 pad_maximum_fusion
  44.8 0.3 fusion.5
  45.1 0.2 fusion.20
  45.3 0.1 fusion.15
  45.4 0.1 copy.18
  45.5 0.2 fusion.12
  45.7 11.7 %pmax.7 = f32[1,4,2]{1,2,0:T(2,128)S(1)} all-reduce(f32[1,4,2]{1,2,0:T(2,128)S(1)} %bitcast.81), channel_id=1, replica_groups=mesh['gr'=2,'sp'=4,'tp'=4] {'sp'}, use_global_device_ids=true, to_apply=%region_1.0 | all-reduce | flops 8 | bytes 64 | tf_op jit(solution)/shard_map/pmax | solution.py:65
  57.4 0.1 copy.20
  57.5 0.1 copy.19
  57.6 0.0 copy-start.2
  57.6 0.0 copy-start.3
  57.6 4.4 %fusion.6 = bf16[768,512]{0,1:T(8,128)(2,1)S(1)} fusion(bf16[2048,512]{1,0:T(8,128)(2,1)} %param.9, bf16[1,768,2048]{2,1,0:T(8,128)(2,1)} %all-gather.2.cloned.1.call-done), kind=kOutput, calls=%fused_computation.9 | convolution fusion | flops 1611005952 | bytes 6029312 | tf_op jit(solution)/shard_map/dot_general | solution.py:52
  62.0 0.0 copy-start.1
  62.0 0.9 copy-done.1
  62.9 0.3 fusion.9
  63.2 8.5 %all-reduce = (f32[1,4,2,128]{3,2,1,0:T(2,128)S(1)}, f32[4,2]{0,1:T(2,128)S(1)}) all-reduce(f32[1,4,2,128]{3,2,1,0:T(2,128)S(1)} %fusion.9, f32[4,2]{0,1:T(2,128)S(1)} %get-tuple-element.17), channel_id=1, replica_groups=mesh['gr'=2,'sp'=4,'tp'=4] {'sp'}, use_global_device_ids=true, to_apply=%region_2.0 | all-reduce | flops 1032 | bytes 8256 | tf_op jit(solution)/shard_map/psum | solution.py:67
  71.7 0.1 copy.21
  71.8 0.1 broadcast_divide_fusion
  71.9 0.0 copy-done.2
  71.9 0.2 multiply_reduce_fusion
  72.1 0.1 mul.157
  72.2 0.1 mul.163
  72.3 0.0 copy-done.3
  72.3 2.0 %fusion.21 = f32[1,2048]{1,0:T(1,128)S(1)} fusion(bf16[512,1]{0,1:T(2,128)(2,1)S(1)} %reshape.244, bf16[512,2048]{1,0:T(8,128)(2,1)} %param.13), kind=kOutput, calls=%fused_computation.37 | convolution fusion | flops 2097152 | bytes 2106368 | tf_op jit(solution)/shard_map/dot_general | solution.py:69
  74.3 1.1 %reshape_bitcast_fusion = bf16[2048,1]{1,0:T(8,128)(2,1)} fusion(bf16[2048]{0:T(1024)(128)(2,1)S(1)} %convert_element_type.40), kind=kLoop, calls=%fused_computation.13 | loop fusion | bytes 8192
  75.4 0.0 reduce-scatter.4.cloned.1.call-update
  75.4 2.3 %copy.24 = bf16[1,768,512]{2,1,0:T(8,128)(2,1)} copy(bf16[1,768,512]{1,2,0:T(8,128)(2,1)} %bitcast.74) | data formatting | bytes 1572864
  77.7 1.2 %copy.23 = bf16[1,768,512]{2,1,0:T(8,128)(2,1)} copy(bf16[1,768,512]{1,2,0:T(8,128)(2,1)S(1)} %bitcast.71) | data formatting | bytes 1572864
  78.9 17.0 %reduce-scatter.4.cloned.1.call-done = bf16[512,1]{1,0:T(8,128)(2,1)} async-done(((bf16[2048,1]{1,0:T(8,128)(2,1)}), bf16[512,1]{1,0:T(8,128)(2,1)}) %reduce-scatter.4.cloned.1.call-update) | async-done | bytes 1040
  95.9 1.6 %copy.29 = bf16[1,512]{1,0:T(2,128)(2,1)} copy(bf16[1,512]{0,1:T(8,128)(2,1)} %bitcast.75) | data formatting | bytes 2048
  (8 shorter events, 0.1 us)
Async XLA Ops:
  7.2 33.6 %copy-start = (bf16[2048,512]{1,0:T(8,128)(2,1)S(1)}, bf16[2048,512]{1,0:T(8,128)(2,1)}, u32[]{:S(2)}) copy-start(bf16[2048,512]{1,0:T(8,128)(2,1)} %param.8) | copy-start | bytes 6291460
  7.2 33.6 %all-gather.2.cloned.1.call-start = ((), (), s32[]{:S(2)}) async-start(), calls=%async_computation.1 | async-start | bytes 3932160 | tf_op jit(solution)/shard_map/all_gather | solution.py:47
  7.9 88.0 %reduce-scatter.4.cloned.1.call-start = ((), (), s32[]{:S(2)}) async-start(), calls=%async_computation.2 | async-start | bytes 655360
  57.6 14.3 %copy-start.2 = (f32[4]{0:T(128)S(1)}, f32[4]{0:T(128)}, u32[]{:S(2)}) copy-start(f32[4]{0:T(128)} %param.11) | copy-start | bytes 52
  57.6 14.7 %copy-start.3 = (f32[128]{0:T(128)S(1)}, f32[128]{0:T(128)}, u32[]{:S(2)}) copy-start(f32[128]{0:T(128)} %param.12) | copy-start | bytes 1540
  62.0 0.9 copy-start.1
Sparse Core Ops, SparseCore 0:
  9.5 31.2 all-gather.1
  75.6 20.2 reduce-scatter.3
where the time goes:
time: 105 us; the launch traced here: 104 us
  waiting for transfers between devices  49.3 us (47%)
  blocking collectives  20.2 us (19%)
  between operations  14.1 us (13%)
  matrix products  10.7 us (10%)
  local copies, waits for them, and re-layouts  7.68 us (7%)
  other arithmetic  2.29 us (2%)
    all_gather x1, waiting for transfers between devices, on_device(): piece = lax.all_gather(layer_input, 'tp', axis=1, tiled=True)  31.6 us
    unnamed x3, waiting for transfers between devices  17.7 us
    pmax x1, blocking collectives, on_device(): overall = lax.pmax(highest, 'sp')  11.7 us
    psum x1, blocking collectives, on_device(): lax.psum((totals * factor, weighted * factor[..., None]), 'sp')  8.5 us
    unnamed x12, local copies, waits for them, and re-layouts  7.06 us
    dot_general x1, matrix products, on_device(): jnp.dot(flattened, value_weight, preferred_element_type=jnp.float32)  4.41 us
    dot_general x1, matrix products, on_device(): jnp.dot(flattened, key_weight, preferred_element_type=jnp.float32)  3.73 us
  transfers between devices with their start and end apart: 2, of which 2 were waited for; matrix products, arithmetic and copies ran while one was open for 4% of the time, Pallas kernels for 0%

commit v1 on v0

v1 whole, which is shorter than its diff:
```python
import functools

import jax
import jax.numpy as jnp
import numpy as np
from jax import lax
from jax.experimental import pallas as pl
from jax.experimental.pallas import tpu as pltpu
from jax.sharding import PartitionSpec as P

MESH = pl.DeviceIdType.MESH
MAP_ROWS = 16


def kernel(
    n_sp, n_tp, heads, head_dim, chunk,
    x_ref, wk_ref, wv_ref, q_ref, lam_ref, gain_ref, wo_ref, fine_ref, coarse_ref,
    k_ref, v_ref, mix_ref,
    xg, wk, wv, wo, q, lam, gain, fine, coarse, keys, values, stats, part, parts,
    load_sem, out_sem, near_send, near_recv, far_send, far_recv, fwd_send, fwd_recv,
    st_send, st_recv, pt_send, pt_recv,
):
    sp = lax.axis_index("sp")
    tp = lax.axis_index("tp")
    rows = x_ref.shape[1]
    wide = 2 * head_dim
    maps = 2 * heads
    steps = rows // chunk
    chips = n_tp // 2
    partner = tp + 1 - 2 * lax.rem(tp, 2)
    out_cols = mix_ref.shape[1]
    local_coarse = n_tp * steps

    loads = [
        pltpu.make_async_copy(x_ref.at[0], xg.at[tp], load_sem.at[0]),
        pltpu.make_async_copy(wk_ref, wk, load_sem.at[1]),
        pltpu.make_async_copy(wv_ref, wv, load_sem.at[2]),
        pltpu.make_async_copy(fine_ref, fine, load_sem.at[3]),
        pltpu.make_async_copy(
            coarse_ref.at[pl.ds(sp * local_coarse, local_coarse)], coarse, load_sem.at[4]
        ),
        pltpu.make_async_copy(q_ref, q, load_sem.at[5]),
        pltpu.make_async_copy(lam_ref, lam, load_sem.at[6]),
        pltpu.make_async_copy(gain_ref, gain, load_sem.at[7]),
        pltpu.make_async_copy(wo_ref, wo, load_sem.at[8]),
    ]

    barrier = pltpu.get_barrier_semaphore()
    for d in range(1, n_tp):
        pl.semaphore_signal(
            barrier, inc=1, device_id={"tp": lax.rem(tp + d, n_tp)}, device_id_type=MESH
        )
    for d in range(1, n_sp):
        pl.semaphore_signal(
            barrier, inc=1, device_id={"sp": lax.rem(sp + d, n_sp)}, device_id_type=MESH
        )
    for load in loads:
        load.start()
    pl.semaphore_wait(barrier, n_tp - 1 + n_sp - 1)

    far = {}
    for j in range(steps):
        for d in range(1, chips):
            far[d, j] = pltpu.make_async_remote_copy(
                src_ref=x_ref.at[0, pl.ds(j * chunk, chunk)],
                dst_ref=xg.at[tp, pl.ds(j * chunk, chunk)],
                send_sem=far_send.at[d - 1, j],
                recv_sem=far_recv.at[d - 1, j],
                device_id={"tp": lax.rem(tp + 2 * d, n_tp)},
                device_id_type=MESH,
            )
            far[d, j].start()
    near = pltpu.make_async_remote_copy(
        src_ref=x_ref.at[0],
        dst_ref=xg.at[tp],
        send_sem=near_send,
        recv_sem=near_recv,
        device_id={"tp": partner},
        device_id_type=MESH,
    )
    near.start()

    lane = lax.broadcasted_iota(jnp.int32, (chunk, wide), 1)
    low_half = lax.rem(lane, head_dim) < head_dim // 2

    def project(block, first, count):
        piece = xg[block, first * chunk:(first + count) * chunk, :]
        raw_keys = jnp.dot(piece, wk[...], preferred_element_type=jnp.float32)
        raw_values = jnp.dot(piece, wv[...], preferred_element_type=jnp.float32)
        values[block, first * chunk:(first + count) * chunk, :] = raw_values.astype(jnp.bfloat16)
        for i in range(count):
            base = coarse[block * steps + first + i]
            base_cos, base_sin = base[0:1, :], base[1:2, :]
            cosine = base_cos * fine[0] - base_sin * fine[1]
            sine = base_sin * fine[0] + base_cos * fine[1]
            for h in range(heads):
                raw = raw_keys[i * chunk:(i + 1) * chunk, h * wide:(h + 1) * wide]
                ahead = pltpu.roll(raw, wide - head_dim // 2, 1)
                behind = pltpu.roll(raw, head_dim // 2, 1)
                turned = raw * cosine + jnp.where(low_half, ahead, behind) * sine
                keys[
                    block, (first + i) * chunk:(first + i + 1) * chunk, h * wide:(h + 1) * wide
                ] = turned.astype(jnp.bfloat16)

    outs = []

    def put(block, first, count, slot):
        where = pl.ds(first * chunk, count * chunk)
        for held, ref, s in ((keys, k_ref, 0), (values, v_ref, 1)):
            copy = pltpu.make_async_copy(
                held.at[block, where], ref.at[block, where], out_sem.at[s, slot]
            )
            copy.start()
            outs.append(copy)

    for load in loads[:5]:
        load.wait()
    project(tp, 0, steps)
    put(tp, 0, steps, 0)
    near.wait_recv()
    project(partner, 0, steps)
    put(partner, 0, steps, 1)

    forwards = []
    slot = 2
    for j in range(steps):
        for d in range(1, chips):
            source = lax.rem(tp + n_tp - 2 * d, n_tp)
            other = source + 1 - 2 * lax.rem(source, 2)
            far[d, j].wait_recv()
            forward = pltpu.make_async_remote_copy(
                src_ref=xg.at[source, pl.ds(j * chunk, chunk)],
                dst_ref=xg.at[source, pl.ds(j * chunk, chunk)],
                send_sem=fwd_send.at[d - 1, j],
                recv_sem=fwd_recv.at[d - 1, j],
                device_id={"tp": partner},
                device_id_type=MESH,
            )
            forward.start()
            forwards.append(forward)
            project(source, j, 1)
            put(source, j, 1, slot)
            forward.wait_recv()
            project(other, j, 1)
            put(other, j, 1, slot + 1)
            slot += 2

    for load in loads[5:]:
        load.wait()
    map_row = lax.broadcasted_iota(jnp.int32, (MAP_ROWS, q.shape[1]), 0)
    map_col = lax.broadcasted_iota(jnp.int32, (MAP_ROWS, q.shape[1]), 1) // head_dim
    spread = jnp.where(map_row == map_col, q[...].astype(jnp.float32), 0.0).astype(jnp.bfloat16)
    scores = [
        lax.dot_general(
            spread, keys[b], (((1,), (1,)), ((), ())), preferred_element_type=jnp.float32
        ) * head_dim ** (-0.5)
        for b in range(n_tp)
    ]
    highest = functools.reduce(
        jnp.maximum, [jnp.max(s, axis=1, keepdims=True) for s in scores]
    )
    total = jnp.zeros_like(highest)
    read = jnp.zeros((MAP_ROWS, q.shape[1]), jnp.float32)
    for b in range(n_tp):
        weight = jnp.exp(scores[b] - highest)
        total = total + jnp.sum(weight, axis=1, keepdims=True)
        upper = weight.astype(jnp.bfloat16)
        lower = (weight - upper.astype(jnp.float32)).astype(jnp.bfloat16)
        read = read + jnp.dot(upper, values[b], preferred_element_type=jnp.float32)
        read = read + jnp.dot(lower, values[b], preferred_element_type=jnp.float32)
    head_of = lax.broadcasted_iota(jnp.int32, (MAP_ROWS, wide), 0) // 2
    own = jnp.zeros((MAP_ROWS, wide), jnp.float32)
    for h in range(heads):
        own = jnp.where(head_of == h, read[:, h * wide:(h + 1) * wide], own)
    first_lane = lax.broadcasted_iota(jnp.int32, (MAP_ROWS, wide), 1) == 0
    stats[sp, 0] = own[:maps]
    stats[sp, 1] = jnp.where(first_lane, highest, total)[:maps]

    exchanges = []
    for d in range(n_sp - 1, 0, -1):
        copy = pltpu.make_async_remote_copy(
            src_ref=stats.at[sp],
            dst_ref=stats.at[sp],
            send_sem=st_send.at[d - 1],
            recv_sem=st_recv.at[d - 1],
            device_id={"sp": lax.rem(sp + d, n_sp)},
            device_id_type=MESH,
        )
        copy.start()
        exchanges.append(copy)
    for copy in exchanges:
        copy.wait_recv()
    heights = stats[:, 1]
    tops = heights[:, :, 0:1]
    sums = heights[:, :, 1:2]
    factor = jnp.exp(tops - jnp.max(tops, axis=0, keepdims=True))
    totals = jnp.sum(sums * factor, axis=0)
    reads = jnp.sum(stats[:, 0] * factor, axis=0) / totals
    normed = []
    for h in range(heads):
        diff = reads[2 * h:2 * h + 1] - lam[0:1, h:h + 1] * reads[2 * h + 1:2 * h + 2]
        scale = lax.rsqrt(jnp.mean(diff * diff, axis=1, keepdims=True) + 1e-06)
        normed.append(diff * scale * gain[...])
    headed = jnp.concatenate(normed, axis=1)
    headed = jnp.broadcast_to(headed, (MAP_ROWS, headed.shape[1])).astype(jnp.bfloat16)
    partials = jnp.dot(headed, wo[...], preferred_element_type=jnp.float32).astype(jnp.bfloat16)
    for b in range(n_tp):
        part[b] = partials[:, b * out_cols:(b + 1) * out_cols]
    swaps = []
    for d in range(n_tp - 1, 0, -1):
        target = lax.rem(tp + d, n_tp)
        copy = pltpu.make_async_remote_copy(
            src_ref=part.at[target],
            dst_ref=parts.at[d - 1],
            send_sem=pt_send.at[d - 1],
            recv_sem=pt_recv.at[d - 1],
            device_id={"tp": target},
            device_id_type=MESH,
        )
        copy.start()
        swaps.append(copy)
    mixed = part[tp].astype(jnp.float32)
    for copy in swaps:
        copy.wait_recv()
    for d in range(1, n_tp):
        mixed = mixed + parts[d - 1].astype(jnp.float32)
    mix_ref[...] = mixed[0:1].astype(jnp.bfloat16)

    near.wait_send()
    for copy in list(far.values()) + forwards + exchanges + swaps:
        copy.wait_send()
    for copy in outs:
        copy.wait()


def tables(length, chunk, head_dim):
    inverse = 1.0 / 10000.0 ** (np.arange(0, head_dim, 2) / head_dim)
    inverse = np.tile(inverse, 4)
    sign = np.tile(np.repeat([-1.0, 1.0], head_dim // 2), 2)

    def pair(positions, axis):
        angles = positions[:, None] * inverse[None, :]
        both = np.stack([np.cos(angles), np.sin(angles) * sign], axis=axis)
        return both.astype(np.float32)

    return pair(np.arange(chunk), 0), pair(np.arange(0, length, chunk), 1)


def on_device(n_sp, n_tp, x, key_weight, value_weight, new_queries, lambdas, head_gain, out_weight):
    heads = lambdas.shape[0]
    columns = key_weight.shape[1]
    head_dim = columns // (2 * heads)
    wide = 2 * head_dim
    seqs, rows, depth = x.shape
    assert seqs == 1
    chunk = rows // 4
    steps = rows // chunk
    chips = n_tp // 2
    out_cols = out_weight.shape[1] // n_tp
    fine, coarse = tables(n_sp * n_tp * rows, chunk, head_dim)
    any_spec = pl.BlockSpec(memory_space=pl.ANY)
    dma = pltpu.SemaphoreType.DMA
    bf16 = jnp.bfloat16
    f32 = jnp.float32
    slots = 2 + 2 * steps * (chips - 1)
    k, v, mixed = pl.pallas_call(
        functools.partial(kernel, n_sp, n_tp, heads, head_dim, chunk),
        out_shape=(
            jax.ShapeDtypeStruct((n_tp, rows, columns), bf16),
            jax.ShapeDtypeStruct((n_tp, rows, columns), bf16),
            jax.ShapeDtypeStruct((1, out_cols), bf16),
        ),
        in_specs=[any_spec] * 9,
        out_specs=(any_spec, any_spec, pl.BlockSpec(memory_space=pltpu.VMEM)),
        scratch_shapes=[
            pltpu.VMEM((n_tp, rows, depth), bf16),
            pltpu.VMEM((depth, columns), bf16),
            pltpu.VMEM((depth, columns), bf16),
            pltpu.VMEM(out_weight.shape, bf16),
            pltpu.VMEM((1, columns), bf16),
            pltpu.VMEM((1, heads), f32),
            pltpu.VMEM((1, wide), f32),
            pltpu.VMEM((2, chunk, wide), f32),
            pltpu.VMEM((n_tp * steps, 2, wide), f32),
            pltpu.VMEM((n_tp, rows, columns), bf16),
            pltpu.VMEM((n_tp, rows, columns), bf16),
            pltpu.VMEM((n_sp, 2, 2 * heads, wide), f32),
            pltpu.VMEM((n_tp, MAP_ROWS, out_cols), bf16),
            pltpu.VMEM((n_tp - 1, MAP_ROWS, out_cols), bf16),
            dma((9,)),
            dma((2, slots)),
            dma,
            dma,
            dma((chips - 1, steps)),
            dma((chips - 1, steps)),
            dma((chips - 1, steps)),
            dma((chips - 1, steps)),
            dma((n_sp - 1,)),
            dma((n_sp - 1,)),
            dma((n_tp - 1,)),
            dma((n_tp - 1,)),
        ],
        compiler_params=pltpu.CompilerParams(
            collective_id=0, has_side_effects=True, vmem_limit_bytes=60 * 1024 * 1024
        ),
    )(
        x, key_weight, value_weight, new_queries, lambdas.reshape(1, heads),
        head_gain.reshape(1, wide), out_weight, jnp.asarray(fine), jnp.asarray(coarse),
    )
    full = (1, n_tp * rows, columns)
    return k.reshape(full), v.reshape(full), mixed


def solution(mesh):
    n_sp, n_tp = mesh.shape["sp"], mesh.shape["tp"]
    in_specs = (
        P("gr", ("sp", "tp"), None),
        P(None, "tp"),
        P(None, "tp"),
        P("gr", "tp"),
        P("tp"),
        P(),
        P("tp", None),
    )
    out_specs = (P("gr", "sp", "tp"), P("gr", "sp", "tp"), P("gr", "tp"))
    return jax.shard_map(
        functools.partial(on_device, n_sp, n_tp),
        mesh=mesh, in_specs=in_specs, out_specs=out_specs, check_vma=False,
    )
```

time: 105 us -> 39.1 us (0.37)
  waiting for transfers between devices: 49.3 us -> 0 us
  Pallas kernels: 0 us -> 34.7 us
  blocking collectives: 20.2 us -> 0 us
  between operations: 14.1 us -> 0.66 us
  matrix products: 10.7 us -> 0 us
  local copies, waits for them, and re-layouts: 7.68 us -> 3.6 us
  other arithmetic: 2.29 us -> 0 us
    pallas_call x0 -> x1, Pallas kernels: none -> 34.7 us  [on_device(): pl.pallas_call(functools.partial(kernel, n_sp, n_tp, heads, head_dim, chu...]
    all_gather x1 -> x0, waiting for transfers between devices: 31.6 us -> none  [on_device(): piece = lax.all_gather(layer_input, 'tp', axis=1, tiled=True)]
    unnamed x3 -> x0, waiting for transfers between devices: 17.7 us -> none
    pmax x1 -> x0, blocking collectives: 11.7 us -> none  [on_device(): overall = lax.pmax(highest, 'sp')]
    dot_general x5 -> x0, matrix products: 10.7 us -> none  [the longest x1 4.41 us: on_device(): jnp.dot(flattened, value_weight, preferred_element_type=jnp.float32)]
    psum x1 -> x0, blocking collectives: 8.5 us -> none  [on_device(): lax.psum((totals * factor, weighted * factor[..., None]), 'sp')]
    unnamed x12 -> x7, local copies, waits for them, and re-layouts: 7.06 us -> 3.6 us
  transfers between devices with their start and end apart: 2 -> 0, of which waited for: 2 -> 0; matrix products, arithmetic and copies ran while one was open for 4% -> 0% of each run, Pallas kernels for 0% -> 0%
where the time goes in v1:
time: 39.1 us; the launch traced here: 39 us
  Pallas kernels  34.7 us (89%)
  local copies, waits for them, and re-layouts  3.6 us (9%)
  between operations  0.66 us (2%)
    pallas_call x1, Pallas kernels, on_device(): pl.pallas_call(functools.partial(kernel, n_sp, n_tp, heads, head_dim, chu...  34.7 us
    unnamed x7, local copies, waits for them, and re-layouts  3.6 us

profile of v1, /device:TPU:0, one launch (start us, length us, event | category | flops | bytes accessed | tf_op | source)
XLA Modules:
  0.0 39.0 jit_solution(17331891254042217872)
XLA Ops:
  0.6 34.7 %shard_map.112 = (bf16[4,192,512]{2,1,0:T(8,128)(2,1)}, bf16[4,192,512]{2,1,0:T(8,128)(2,1)}, bf16[1,512]{1,0:T(2,128)(2,1)}) custom-call(bf16[1,192,2048]{2,1,0:T(8,128)(2,1)} %x_ref.1, bf16[2048,512]{1,0:T(8,128)(2,1)} %wk_ref.1, bf16[2048,512]{1,0:T(8,128)(2,1)} %wv_ref.1, bf16[1,512]{1,0:T(2,128)(2,1)} %q_ref.1, f32[1,4]{1,0:T(1,128)} %bitcast.6, ...), custom_call_target="tpu_custom_call" | custom-call | tf_op jit(solution)/shard_map/pallas_call | solution.py:266
  35.4 0.0 copy-start
  35.4 0.0 copy-start.1
  35.4 2.1 %copy.15 = bf16[1,768,512]{2,1,0:T(8,128)(2,1)} copy(bf16[1,768,512]{2,1,0:T(8,128)(2,1)} %bitcast.5) | data formatting | bytes 1572864
  37.5 0.0 copy-done
  37.5 0.9 %copy.16 = bf16[1,768,512]{2,1,0:T(8,128)(2,1)} copy(bf16[1,768,512]{2,1,0:T(8,128)(2,1)S(1)} %bitcast.4) | data formatting | bytes 1572864
  38.4 0.0 copy-done.1
  38.4 0.6 %copy.17 = bf16[1,512]{1,0:T(2,128)(2,1)} copy(bf16[1,512]{1,0:T(2,128)(2,1)S(1)} %copy-done.1) | data formatting | bytes 2048
Async XLA Ops:
  35.4 2.2 %copy-start = (bf16[4,192,512]{2,1,0:T(8,128)(2,1)S(1)}, bf16[4,192,512]{2,1,0:T(8,128)(2,1)}, u32[]{:S(2)}) copy-start(bf16[4,192,512]{2,1,0:T(8,128)(2,1)} %get-tuple-element.7) | copy-start | bytes 2359300
  35.4 3.0 %copy-start.1 = (bf16[1,512]{1,0:T(2,128)(2,1)S(1)}, bf16[1,512]{1,0:T(2,128)(2,1)}, u32[]{:S(2)}) copy-start(bf16[1,512]{1,0:T(2,128)(2,1)} %get-tuple-element.14) | copy-start | bytes 3076

commit v2 on v1

--- a/solution.py
+++ b/solution.py
@@ -10,14 +10,16 @@
 
 MESH = pl.DeviceIdType.MESH
 MAP_ROWS = 16
+VMEM_BYTES = 67043328
+SMALL_BYTES = 16384
 
 
 def kernel(
     n_sp, n_tp, heads, head_dim, chunk,
     x_ref, wk_ref, wv_ref, q_ref, lam_ref, gain_ref, wo_ref, fine_ref, coarse_ref,
-    k_ref, v_ref, mix_ref,
-    xg, wk, wv, wo, q, lam, gain, fine, coarse, keys, values, stats, part, parts,
-    load_sem, out_sem, near_send, near_recv, far_send, far_recv, fwd_send, fwd_recv,
+    keys, values, mix_ref,
+    xg, wk, wv, wo, q, lam, gain, fine, coarse, stats, part, parts,
+    load_sem, up_sem, down_sem, near_send, near_recv, far_send, far_recv, fwd_send, fwd_recv,
     st_send, st_recv, pt_send, pt_recv,
 ):
     sp = lax.axis_index("sp")
@@ -32,6 +34,7 @@
     local_coarse = n_tp * steps
 
     loads = [
+        pltpu.make_async_copy(q_ref, q, load_sem.at[5]),
         pltpu.make_async_copy(x_ref.at[0], xg.at[tp], load_sem.at[0]),
         pltpu.make_async_copy(wk_ref, wk, load_sem.at[1]),
         pltpu.make_async_copy(wv_ref, wv, load_sem.at[2]),
@@ -39,7 +42,6 @@
         pltpu.make_async_copy(
             coarse_ref.at[pl.ds(sp * local_coarse, local_coarse)], coarse, load_sem.at[4]
         ),
-        pltpu.make_async_copy(q_ref, q, load_sem.at[5]),
         pltpu.make_async_copy(lam_ref, lam, load_sem.at[6]),
         pltpu.make_async_copy(gain_ref, gain, load_sem.at[7]),
         pltpu.make_async_copy(wo_ref, wo, load_sem.at[8]),
@@ -50,13 +52,20 @@
         pl.semaphore_signal(
             barrier, inc=1, device_id={"tp": lax.rem(tp + d, n_tp)}, device_id_type=MESH
         )
-    for d in range(1, n_sp):
-        pl.semaphore_signal(
-            barrier, inc=1, device_id={"sp": lax.rem(sp + d, n_sp)}, device_id_type=MESH
-        )
+    has_lower = sp > 0
+    has_upper = sp < n_sp - 1
+
+    @pl.when(has_lower)
+    def _():
+        pl.semaphore_signal(barrier, inc=1, device_id={"sp": sp - 1}, device_id_type=MESH)
+
+    @pl.when(has_upper)
+    def _():
+        pl.semaphore_signal(barrier, inc=1, device_id={"sp": sp + 1}, device_id_type=MESH)
+
     for load in loads:
         load.start()
-    pl.semaphore_wait(barrier, n_tp - 1 + n_sp - 1)
+    pl.semaphore_wait(barrier, n_tp - 1 + jnp.where(has_lower, 1, 0) + jnp.where(has_upper, 1, 0))
 
     far = {}
     for j in range(steps):
@@ -80,6 +89,17 @@
     )
     near.start()
 
+    pl.when(has_lower)(lambda: pl.semaphore_wait(up_sem, 1))
+
+    @pl.when(has_upper)
+    def _():
+        pl.semaphore_signal(up_sem, inc=1, device_id={"sp": sp + 1}, device_id_type=MESH)
+        pl.semaphore_wait(down_sem, 1)
+
+    @pl.when(has_lower)
+    def _():
+        pl.semaphore_signal(down_sem, inc=1, device_id={"sp": sp - 1}, device_id_type=MESH)
+
     lane = lax.broadcasted_iota(jnp.int32, (chunk, wide), 1)
     low_half = lax.rem(lane, head_dim) < head_dim // 2
 
@@ -102,27 +122,43 @@
                     block, (first + i) * chunk:(first + i + 1) * chunk, h * wide:(h + 1) * wide
                 ] = turned.astype(jnp.bfloat16)
 
-    outs = []
-
-    def put(block, first, count, slot):
-        where = pl.ds(first * chunk, count * chunk)
-        for held, ref, s in ((keys, k_ref, 0), (values, v_ref, 1)):
-            copy = pltpu.make_async_copy(
-                held.at[block, where], ref.at[block, where], out_sem.at[s, slot]
-            )
-            copy.start()
-            outs.append(copy)
-
-    for load in loads[:5]:
+    for load in loads[:6]:
         load.wait()
+    map_row = lax.broadcasted_iota(jnp.int32, (MAP_ROWS, q.shape[1]), 0)
+    map_col = lax.broadcasted_iota(jnp.int32, (MAP_ROWS, q.shape[1]), 1) // head_dim
+    spread = jnp.where(map_row == map_col, q[...].astype(jnp.float32), 0.0).astype(jnp.bfloat16)
+
+    def attend(state, block, first, count):
+        where = slice(first * chunk, (first + count) * chunk)
+        score = lax.dot_general(
+            spread, keys[block, where, :], (((1,), (1,)), ((), ())),
+            preferred_element_type=jnp.float32,
+        ) * head_dim ** (-0.5)
+        highest = jnp.max(score, axis=1, keepdims=True)
+        if state is not None:
+            highest = jnp.maximum(highest, state[0])
+        weight = jnp.exp(score - highest)
+        total = jnp.sum(weight, axis=1, keepdims=True)
+        upper = weight.astype(jnp.bfloat16)
+        lower = (weight - upper.astype(jnp.float32)).astype(jnp.bfloat16)
+        read = jnp.dot(
+            jnp.concatenate([upper, lower], axis=0), values[block, where, :],
+            preferred_element_type=jnp.float32,
+        )
+        read = read[:MAP_ROWS] + read[MAP_ROWS:]
+        if state is not None:
+            fade = jnp.exp(state[0] - highest)
+            total = total + state[1] * fade
+            read = read + state[2] * fade
+        return highest, total, read
+
     project(tp, 0, steps)
-    put(tp, 0, steps, 0)
+    state = attend(None, tp, 0, steps)
     near.wait_recv()
     project(partner, 0, steps)
-    put(partner, 0, steps, 1)
+    state = attend(state, partner, 0, steps)
 
     forwards = []
-    slot = 2
     for j in range(steps):
         for d in range(1, chips):
             source = lax.rem(tp + n_tp - 2 * d, n_tp)
@@ -139,35 +175,14 @@
             forward.start()
             forwards.append(forward)
             project(source, j, 1)
-            put(source, j, 1, slot)
+            state = attend(state, source, j, 1)
             forward.wait_recv()
             project(other, j, 1)
-            put(other, j, 1, slot + 1)
-            slot += 2
-
-    for load in loads[5:]:
+            state = attend(state, other, j, 1)
+
+    for load in loads[6:]:
         load.wait()
-    map_row = lax.broadcasted_iota(jnp.int32, (MAP_ROWS, q.shape[1]), 0)
-    map_col = lax.broadcasted_iota(jnp.int32, (MAP_ROWS, q.shape[1]), 1) // head_dim
-    spread = jnp.where(map_row == map_col, q[...].astype(jnp.float32), 0.0).astype(jnp.bfloat16)
-    scores = [
-        lax.dot_general(
-            spread, keys[b], (((1,), (1,)), ((), ())), preferred_element_type=jnp.float32
-        ) * head_dim ** (-0.5)
-        for b in range(n_tp)
-    ]
-    highest = functools.reduce(
-        jnp.maximum, [jnp.max(s, axis=1, keepdims=True) for s in scores]
-    )
-    total = jnp.zeros_like(highest)
-    read = jnp.zeros((MAP_ROWS, q.shape[1]), jnp.float32)
-    for b in range(n_tp):
-        weight = jnp.exp(scores[b] - highest)
-        total = total + jnp.sum(weight, axis=1, keepdims=True)
-        upper = weight.astype(jnp.bfloat16)
-        lower = (weight - upper.astype(jnp.float32)).astype(jnp.bfloat16)
-        read = read + jnp.dot(upper, values[b], preferred_element_type=jnp.float32)
-        read = read + jnp.dot(lower, values[b], preferred_element_type=jnp.float32)
+    highest, total, read = state
     head_of = lax.broadcasted_iota(jnp.int32, (MAP_ROWS, wide), 0) // 2
     own = jnp.zeros((MAP_ROWS, wide), jnp.float32)
     for h in range(heads):
@@ -229,8 +244,6 @@
     near.wait_send()
     for copy in list(far.values()) + forwards + exchanges + swaps:
         copy.wait_send()
-    for copy in outs:
-        copy.wait()
 
 
 def tables(length, chunk, head_dim):
@@ -258,20 +271,20 @@
     chips = n_tp // 2
     out_cols = out_weight.shape[1] // n_tp
     fine, coarse = tables(n_sp * n_tp * rows, chunk, head_dim)
-    any_spec = pl.BlockSpec(memory_space=pl.ANY)
+    hbm_spec = pl.BlockSpec(memory_space=pltpu.HBM)
     dma = pltpu.SemaphoreType.DMA
     bf16 = jnp.bfloat16
     f32 = jnp.float32
-    slots = 2 + 2 * steps * (chips - 1)
+    room = 2 * n_tp * rows * columns * 2 + SMALL_BYTES
     k, v, mixed = pl.pallas_call(
         functools.partial(kernel, n_sp, n_tp, heads, head_dim, chunk),
         out_shape=(
-            jax.ShapeDtypeStruct((n_tp, rows, columns), bf16),
-            jax.ShapeDtypeStruct((n_tp, rows, columns), bf16),
+            pltpu.VMEM((n_tp, rows, columns), bf16),
+            pltpu.VMEM((n_tp, rows, columns), bf16),
             jax.ShapeDtypeStruct((1, out_cols), bf16),
         ),
-        in_specs=[any_spec] * 9,
-        out_specs=(any_spec, any_spec, pl.BlockSpec(memory_space=pltpu.VMEM)),
+        in_specs=[hbm_spec] * 9,
+        out_specs=(pl.BlockSpec(memory_space=pltpu.VMEM),) * 3,
         scratch_shapes=[
             pltpu.VMEM((n_tp, rows, depth), bf16),
             pltpu.VMEM((depth, columns), bf16),
@@ -282,13 +295,12 @@
             pltpu.VMEM((1, wide), f32),
             pltpu.VMEM((2, chunk, wide), f32),
             pltpu.VMEM((n_tp * steps, 2, wide), f32),
-            pltpu.VMEM((n_tp, rows, columns), bf16),
-            pltpu.VMEM((n_tp, rows, columns), bf16),
             pltpu.VMEM((n_sp, 2, 2 * heads, wide), f32),
             pltpu.VMEM((n_tp, MAP_ROWS, out_cols), bf16),
             pltpu.VMEM((n_tp - 1, MAP_ROWS, out_cols), bf16),
             dma((9,)),
-            dma((2, slots)),
+            pltpu.SemaphoreType.REGULAR,
+            pltpu.SemaphoreType.REGULAR,
             dma,
             dma,
             dma((chips - 1, steps)),
@@ -301,7 +313,7 @@
             dma((n_tp - 1,)),
         ],
         compiler_params=pltpu.CompilerParams(
-            collective_id=0, has_side_effects=True, vmem_limit_bytes=60 * 1024 * 1024
+            collective_id=0, has_side_effects=True, vmem_limit_bytes=VMEM_BYTES - room
         ),
     )(
         x, key_weight, value_weight, new_queries, lambdas.reshape(1, heads),

time: 39.1 us -> 37.2 us (0.951)
  local copies, waits for them, and re-layouts: 3.6 us -> 2.34 us
  Pallas kernels: 34.7 us -> 34.1 us
    unnamed x7 -> x5, local copies, waits for them, and re-layouts: 3.6 us -> 2.34 us
    pallas_call x1, Pallas kernels: 34.7 us -> 34.1 us  [on_device(): pl.pallas_call(functools.partial(kernel, n_sp, n_tp, heads, head_dim, chu...]
where the time goes in v2:
time: 37.2 us; the launch traced here: 37.1 us
  Pallas kernels  34.1 us (92%)
  local copies, waits for them, and re-layouts  2.34 us (6%)
  between operations  0.65 us (2%)
    pallas_call x1, Pallas kernels, on_device(): pl.pallas_call(functools.partial(kernel, n_sp, n_tp, heads, head_dim, chu...  34.1 us
    unnamed x5, local copies, waits for them, and re-layouts  2.34 us

profile of v2, /device:TPU:0, one launch (start us, length us, event | category | flops | bytes accessed | tf_op | source)
XLA Modules:
  0.0 37.1 jit_solution(18129337904058001581)
XLA Ops:
  0.6 34.1 %shard_map.112 = (bf16[4,192,512]{2,1,0:T(8,128)(2,1)S(1)}, bf16[4,192,512]{2,1,0:T(8,128)(2,1)S(1)}, bf16[1,512]{1,0:T(2,128)(2,1)}) custom-call(bf16[1,192,2048]{2,1,0:T(8,128)(2,1)} %x_ref.1, bf16[2048,512]{1,0:T(8,128)(2,1)} %wk_ref.1, bf16[2048,512]{1,0:T(8,128)(2,1)} %wv_ref.1, bf16[1,512]{1,0:T(2,128)(2,1)} %q_ref.1, f32[1,4]{1,0:T(1,128)} %bitcast.6, ...), custom_call_target="tpu_custom_call" | custom-call | tf_op jit(solution)/shard_map/pallas_call | solution.py:279
  34.7 0.0 copy-start
  34.7 0.9 %copy.15 = bf16[1,768,512]{2,1,0:T(8,128)(2,1)} copy(bf16[1,768,512]{2,1,0:T(8,128)(2,1)S(1)} %bitcast.5) | data formatting | bytes 1572864
  35.6 0.9 %copy.16 = bf16[1,768,512]{2,1,0:T(8,128)(2,1)} copy(bf16[1,768,512]{2,1,0:T(8,128)(2,1)S(1)} %bitcast.4) | data formatting | bytes 1572864
  36.5 0.0 copy-done
  36.5 0.6 %copy.17 = bf16[1,512]{1,0:T(2,128)(2,1)} copy(bf16[1,512]{1,0:T(2,128)(2,1)S(1)} %copy-done) | data formatting | bytes 2048
Async XLA Ops:
  34.7 1.8 %copy-start = (bf16[1,512]{1,0:T(2,128)(2,1)S(1)}, bf16[1,512]{1,0:T(2,128)(2,1)}, u32[]{:S(2)}) copy-start(bf16[1,512]{1,0:T(2,128)(2,1)} %get-tuple-element.17) | copy-start | bytes 3076

commit v3 on v2

--- a/solution.py
+++ b/solution.py
@@ -33,9 +33,9 @@
     out_cols = mix_ref.shape[1]
     local_coarse = n_tp * steps
 
+    own_load = pltpu.make_async_copy(x_ref.at[0], xg.at[tp], load_sem.at[0])
     loads = [
         pltpu.make_async_copy(q_ref, q, load_sem.at[5]),
-        pltpu.make_async_copy(x_ref.at[0], xg.at[tp], load_sem.at[0]),
         pltpu.make_async_copy(wk_ref, wk, load_sem.at[1]),
         pltpu.make_async_copy(wv_ref, wv, load_sem.at[2]),
         pltpu.make_async_copy(fine_ref, fine, load_sem.at[3]),
@@ -47,6 +47,7 @@
         pltpu.make_async_copy(wo_ref, wo, load_sem.at[8]),
     ]
 
+    own_load.start()
     barrier = pltpu.get_barrier_semaphore()
     for d in range(1, n_tp):
         pl.semaphore_signal(
@@ -63,15 +64,14 @@
     def _():
         pl.semaphore_signal(barrier, inc=1, device_id={"sp": sp + 1}, device_id_type=MESH)
 
-    for load in loads:
-        load.start()
     pl.semaphore_wait(barrier, n_tp - 1 + jnp.where(has_lower, 1, 0) + jnp.where(has_upper, 1, 0))
 
+    own_load.wait()
     far = {}
     for j in range(steps):
         for d in range(1, chips):
             far[d, j] = pltpu.make_async_remote_copy(
-                src_ref=x_ref.at[0, pl.ds(j * chunk, chunk)],
+                src_ref=xg.at[tp, pl.ds(j * chunk, chunk)],
                 dst_ref=xg.at[tp, pl.ds(j * chunk, chunk)],
                 send_sem=far_send.at[d - 1, j],
                 recv_sem=far_recv.at[d - 1, j],
@@ -80,13 +80,15 @@
             )
             far[d, j].start()
     near = pltpu.make_async_remote_copy(
-        src_ref=x_ref.at[0],
+        src_ref=xg.at[tp],
         dst_ref=xg.at[tp],
         send_sem=near_send,
         recv_sem=near_recv,
         device_id={"tp": partner},
         device_id_type=MESH,
     )
+    for load in loads:
+        load.start()
     near.start()
 
     pl.when(has_lower)(lambda: pl.semaphore_wait(up_sem, 1))
@@ -122,7 +124,7 @@
                     block, (first + i) * chunk:(first + i + 1) * chunk, h * wide:(h + 1) * wide
                 ] = turned.astype(jnp.bfloat16)
 
-    for load in loads[:6]:
+    for load in loads[:5]:
         load.wait()
     map_row = lax.broadcasted_iota(jnp.int32, (MAP_ROWS, q.shape[1]), 0)
     map_col = lax.broadcasted_iota(jnp.int32, (MAP_ROWS, q.shape[1]), 1) // head_dim
@@ -180,7 +182,7 @@
             project(other, j, 1)
             state = attend(state, other, j, 1)
 
-    for load in loads[6:]:
+    for load in loads[5:]:
         load.wait()
     highest, total, read = state
     head_of = lax.broadcasted_iota(jnp.int32, (MAP_ROWS, wide), 0) // 2

time: 37.2 us -> 37 us (level)
  no operation moved by 1% of the time
where the time goes in v3:
time: 37 us; the launch traced here: 36.9 us
  Pallas kernels  33.9 us (92%)
  local copies, waits for them, and re-layouts  2.34 us (6%)
  between operations  0.65 us (2%)
    pallas_call x1, Pallas kernels, on_device(): pl.pallas_call(functools.partial(kernel, n_sp, n_tp, heads, head_dim, chu...  33.9 us
    unnamed x5, local copies, waits for them, and re-layouts  2.34 us

profile of v3, /device:TPU:0, one launch (start us, length us, event | category | flops | bytes accessed | tf_op | source)
XLA Modules:
  0.0 36.9 jit_solution(2789621203862307661)
XLA Ops:
  0.6 33.9 %shard_map.112 = (bf16[4,192,512]{2,1,0:T(8,128)(2,1)S(1)}, bf16[4,192,512]{2,1,0:T(8,128)(2,1)S(1)}, bf16[1,512]{1,0:T(2,128)(2,1)}) custom-call(bf16[1,192,2048]{2,1,0:T(8,128)(2,1)} %x_ref.1, bf16[2048,512]{1,0:T(8,128)(2,1)} %wk_ref.1, bf16[2048,512]{1,0:T(8,128)(2,1)} %wv_ref.1, bf16[1,512]{1,0:T(2,128)(2,1)} %q_ref.1, f32[1,4]{1,0:T(1,128)} %bitcast.6, ...), custom_call_target="tpu_custom_call" | custom-call | tf_op jit(solution)/shard_map/pallas_call | solution.py:281
  34.5 0.0 copy-start
  34.5 0.9 %copy.15 = bf16[1,768,512]{2,1,0:T(8,128)(2,1)} copy(bf16[1,768,512]{2,1,0:T(8,128)(2,1)S(1)} %bitcast.5) | data formatting | bytes 1572864
  35.4 0.9 %copy.16 = bf16[1,768,512]{2,1,0:T(8,128)(2,1)} copy(bf16[1,768,512]{2,1,0:T(8,128)(2,1)S(1)} %bitcast.4) | data formatting | bytes 1572864
  36.3 0.0 copy-done
  36.3 0.6 %copy.17 = bf16[1,512]{1,0:T(2,128)(2,1)} copy(bf16[1,512]{1,0:T(2,128)(2,1)S(1)} %copy-done) | data formatting | bytes 2048
Async XLA Ops:
  34.5 1.8 %copy-start = (bf16[1,512]{1,0:T(2,128)(2,1)S(1)}, bf16[1,512]{1,0:T(2,128)(2,1)}, u32[]{:S(2)}) copy-start(bf16[1,512]{1,0:T(2,128)(2,1)} %get-tuple-element.17) | copy-start | bytes 3076
